TPU v7x, 32 devices: a whole 2x2x4 slice. The times are simulated.
32 devices in a mesh: sp: 8 (over z, x), tp: 4 (over y, core).
Axes of the slice: x: 2, y: 2, z: 4, core: 2. Of those that a mesh axis runs over, the one named last changes fastest.
Arguments:
- residual: bfloat16 [2048, 2048], P(('sp', 'tp')), may hold values from -6 to 6
- first_query: bfloat16 [2048, 512], P('sp', 'tp'), may hold values from -6 to 6
- second_query: bfloat16 [2048, 512], P('sp', 'tp'), may hold values from -6 to 6
- first_key: bfloat16 [2048, 512], P('sp', 'tp'), may hold values from -6 to 6
- second_key: bfloat16 [2048, 512], P('sp', 'tp'), may hold values from -6 to 6
- values: bfloat16 [2048, 1024], P('sp', 'tp'), may hold values from -6 to 6
- lambdas: float32 [8], P('tp'), may hold values from 0.3 to 0.8
- head_gain: float32 [128], replicated, may hold values from 0.1 to 1.9
- out_weight: bfloat16 [1024, 2048], P('tp'), may hold values from -0.1875 to 0.1875
- norm_gain: float32 [2048], replicated, may hold values from 0.1 to 1.9
- up_weight: bfloat16 [2048, 4096], P('sp', 'tp'), may hold values from -0.125 to 0.125
- down_weight: bfloat16 [4096, 2048], P('tp', 'sp'), may hold values from -0.09375 to 0.09375
Outputs:
- mixed: bfloat16 [2048, 2048], P(('sp', 'tp'))
All inputs are finite; a program needn't handle non-finite values.
Results may differ from a plain program's by a relative error of at most 0.019.
Values may be sent and summed in bfloat16 or wider, within the bound.
A program may use at most 128 MiB of HBM per device.

v0:
```python
import jax
import jax.numpy as jnp
from jax import lax
from jax.sharding import PartitionSpec as P


def rotate(blocked, positions):
    half = blocked.shape[-1] // 2
    inverse = 10000.0 ** (-jnp.arange(0, half, dtype=jnp.float32) * 2.0 / blocked.shape[-1])
    angle = positions[:, None] * inverse[None, :]
    cosine = jnp.cos(angle)[:, None, :]
    sine = jnp.sin(angle)[:, None, :]
    first, second = (blocked[..., :half], blocked[..., half:])
    return jnp.concatenate(
        [first * cosine - second * sine, second * cosine + first * sine], axis=-1
    )


def absorb(state, queries, keys, vals, factor):
    top, total, summed = state
    scores = jnp.einsum("qhe,khe->qhk", queries, keys, preferred_element_type=jnp.float32) * factor
    peak = jnp.maximum(top, jnp.max(scores, axis=-1))
    shrink = jnp.exp(top - peak)
    weights = jnp.exp(scores - peak[..., None])
    total = total * shrink + jnp.sum(weights, axis=-1)
    summed = summed * shrink[..., None] + jnp.einsum(
        "qhk,khe->qhe", weights.astype(jnp.bfloat16), vals, preferred_element_type=jnp.float32
    )
    return (peak, total, summed)


def layer_norm(stream, gain):
    center = stream - jnp.mean(stream, axis=-1, keepdims=True)
    spread = jnp.mean(center * center, axis=-1, keepdims=True)
    return center * lax.rsqrt(spread + 1e-05) * gain


def local(
    residual,
    first_query,
    second_query,
    first_key,
    second_key,
    values,
    lambdas,
    head_gain,
    out_weight,
    norm_gain,
    up_weight,
    down_weight,
):
    local_rows = first_query.shape[0]
    head_count = lambdas.shape[0]
    head_width = first_query.shape[1] // head_count
    value_width = values.shape[1] // head_count
    quarter_rows = local_rows // lax.axis_size("tp")
    factor = head_width ** (-0.5)
    positions = (lax.axis_index("sp") * local_rows + jnp.arange(local_rows)).astype(jnp.float32)

    def prepare(source):
        turned = rotate(
            source.astype(jnp.float32).reshape(local_rows, head_count, head_width), positions
        )
        return turned.astype(jnp.bfloat16)

    query_a, query_b = (prepare(first_query), prepare(second_query))
    key_a = prepare(first_key).reshape(local_rows, head_count * head_width)
    key_b = prepare(second_key).reshape(local_rows, head_count * head_width)
    start_state = (
        jnp.full((local_rows, head_count), -1e30, jnp.float32),
        jnp.zeros((local_rows, head_count), jnp.float32),
        jnp.zeros((local_rows, head_count, value_width), jnp.float32),
    )
    piece_a = lax.all_gather(key_a, "sp", axis=0, tiled=True)
    piece_b = lax.all_gather(key_b, "sp", axis=0, tiled=True)
    piece_v = lax.all_gather(values, "sp", axis=0, tiled=True)
    count = piece_a.shape[0]
    block = 512
    blocks = count // block

    def advance(state, item):
        block_a, block_b, block_v = item
        return (
            (
                absorb(state[0], query_a, block_a, block_v, factor),
                absorb(state[1], query_b, block_b, block_v, factor),
            ),
            None,
        )

    items = (
        piece_a.reshape(blocks, block, head_count, head_width),
        piece_b.reshape(blocks, block, head_count, head_width),
        piece_v.reshape(blocks, block, head_count, value_width),
    )
    state_a, state_b = lax.scan(advance, (start_state, start_state), items)[0]
    diff = state_a[2] / state_a[1][..., None] - lambdas[None, :, None] * (
        state_b[2] / state_b[1][..., None]
    )
    scale = lax.rsqrt(jnp.mean(diff * diff, axis=-1, keepdims=True) + 1e-05)
    flat = (
        (diff * scale * head_gain * 0.8)
        .astype(jnp.bfloat16)
        .reshape(local_rows, head_count * value_width)
    )
    projected = lax.psum(
        jnp.dot(flat, out_weight, preferred_element_type=jnp.float32).astype(jnp.bfloat16), "tp"
    ).astype(jnp.float32)
    stream = lax.all_gather(residual, "tp", axis=0, tiled=True)
    whole = layer_norm(stream.astype(jnp.float32) + projected, norm_gain).astype(jnp.bfloat16)
    own_normed = lax.dynamic_slice_in_dim(
        whole, lax.axis_index("tp") * quarter_rows, quarter_rows, 0
    )
    lifted = jnp.dot(
        whole,
        lax.all_gather(up_weight, "sp", axis=0, tiled=True),
        preferred_element_type=jnp.float32,
    )
    down_full = lax.all_gather(down_weight, "sp", axis=1, tiled=True)
    hidden = jnp.square(jax.nn.relu(lifted)).astype(jnp.bfloat16)
    lowered = lax.psum_scatter(
        jnp.dot(hidden, down_full, preferred_element_type=jnp.float32).astype(jnp.bfloat16),
        "tp",
        scatter_dimension=0,
        tiled=True,
    ).astype(jnp.float32)
    return (own_normed.astype(jnp.float32) + lowered).astype(jnp.bfloat16)


def solution(mesh):
    in_specs = (
        P(("sp", "tp"), None),
        P("sp", "tp"),
        P("sp", "tp"),
        P("sp", "tp"),
        P("sp", "tp"),
        P("sp", "tp"),
        P("tp"),
        P(),
        P("tp", None),
        P(),
        P("sp", "tp"),
        P("tp", "sp"),
    )
    out_specs = P(("sp", "tp"), None)
    return jax.shard_map(local, mesh=mesh, in_specs=in_specs, out_specs=out_specs, check_vma=False)
```

profile of v0, /device:TPU:0, one launch (start us, length us, event | category | flops | bytes accessed | tf_op | source)
XLA Modules:
  0.0 354.3 jit_solution(2607594345238030326)
XLA Ops:
  6.5 0.7 all-gather.7.cloned.1.call-update
  7.3 0.7 all-gather.5.cloned.1.call-update
  8.1 0.9 copy.21
  9.1 0.9 copy.22
  10.0 0.9 copy.23
  11.0 0.9 copy.24
  11.9 0.2 multiply_cosine_fusion
  12.2 34.2 %all_gather.21 = bf16[2048,128]{0,1:T(8,128)(2,1)S(1)} all-gather(bf16[256,128]{0,1:T(8,128)(2,1)S(1)} %bitcast.66), channel_id=1, replica_groups=mesh['sp'=8,'tp'=4] {'sp'}, dimensions={0}, use_global_device_ids=true | all-gather | bytes 589824 | tf_op jit(solution)/shard_map/all_gather | solution.py:75
  46.4 0.4 reshape.137
  46.8 0.9 copy.27
  47.7 31.6 %all_gather.19 = bf16[2048,128]{0,1:T(8,128)(2,1)S(1)} all-gather(bf16[256,128]{0,1:T(8,128)(2,1)S(1)} %bitcast.67), channel_id=1, replica_groups=mesh['sp'=8,'tp'=4] {'sp'}, dimensions={0}, use_global_device_ids=true | all-gather | bytes 589824 | tf_op jit(solution)/shard_map/all_gather | solution.py:74
  79.3 0.4 reshape.131
  79.7 0.9 copy.25
  80.6 2.1 reshape.134
  82.7 42.6 %while.21 = (s32[]{:T(128)}, f32[256,2]{0,1:T(2,128)S(1)}, f32[256,2]{0,1:T(2,128)}, f32[256,2,128]{0,2,1:T(8,128)}, f32[256,2]{0,1:T(2,128)S(1)}, /*index=5*/f3...) while((s32[]{:T(128)}, f32[256,2]{0,1:T(2,128)S(1)}, ...), condition=%wide.region_5.6_spmd.clone, body=%wide.region_0.5_spmd.clone.sunk | while | flops 204870656 | bytes 9381043 | solution.py:96
  82.7 1.3 fusion.60
  84.0 0.2 fusion.65
  84.2 1.3 fusion.62
  85.5 0.2 fusion.64
  85.6 0.6 fusion.66
  86.3 1.8 constant_dynamic-slice_fusion.2
  88.1 1.1 copy.32
  89.2 1.7 fusion.68
  90.9 1.0 fusion.67
  92.0 1.3 fusion.60
  93.2 0.2 fusion.65
  93.4 1.3 fusion.62
  94.7 0.2 fusion.64
  94.9 1.3 fusion.66
  96.2 1.8 constant_dynamic-slice_fusion.2
  98.0 1.1 copy.32
  99.1 2.0 fusion.68
  101.1 2.0 fusion.67
  103.1 1.3 fusion.60
  104.4 0.2 fusion.65
  104.5 1.3 fusion.62
  105.8 0.2 fusion.64
  106.0 1.3 fusion.66
  107.3 1.8 constant_dynamic-slice_fusion.2
  109.1 1.1 copy.32
  110.2 2.0 fusion.68
  112.2 2.0 fusion.67
  114.2 1.3 fusion.60
  115.7 1.3 fusion.62
  116.9 0.2 fusion.64
  117.1 1.3 fusion.66
  118.4 1.8 constant_dynamic-slice_fusion.2
  120.3 1.1 copy.32
  121.4 2.0 fusion.68
  123.4 2.0 fusion.67
  125.3 1.2 multiply_reduce_fusion.1
  126.5 0.7 multiply_convert_fusion.1
  127.3 1.4 convolution_convert_fusion.1
  128.8 0.5 all-gather.11.cloned.1.call-update
  129.4 0.5 all-gather.9.cloned.1.call-update
  130.0 35.5 %all-reduce.2.cloned.1.call-done = bf16[256,2048]{1,0:T(8,128)(2,1)} async-done(((bf16[256,2048]{1,0:T(8,128)(2,1)}), bf16[256,2048]{1,0:T(8,128)(2,1)}) %all-reduce.2.cloned.1.call-update) | async-done | bytes 1048592 | tf_op jit(solution)/shard_map/psum | solution.py:106
  165.4 2.0 fusion.25
  167.5 0.5 multiply_reduce_fusion
  168.0 0.5 multiply_convert_fusion
  168.5 74.0 %all-gather.11.cloned.1.call-done = bf16[1024,2048]{1,0:T(8,128)(2,1)} async-done(((bf16[1024,256]{1,0:T(8,128)(2,1)}), bf16[1024,2048]{1,0:T(8,128)(2,1)}) %all-gather.11.cloned.1.call-update) | async-done | bytes 4194320 | tf_op jit(solution)/shard_map/all_gather | solution.py:119
  242.5 73.0 %all-gather.9.cloned.1.call-done = bf16[2048,1024]{1,0:T(8,128)(2,1)} async-done(((bf16[256,1024]{1,0:T(8,128)(2,1)}), bf16[2048,1024]{1,0:T(8,128)(2,1)}) %all-gather.9.cloned.1.call-update) | async-done | bytes 4194320 | tf_op jit(solution)/shard_map/all_gather | solution.py:116
  315.5 6.8 %convolution_convert_fusion = bf16[256,2048]{1,0:T(8,128)(2,1)} fusion(bf16[1024,2048]{1,0:T(8,128)(2,1)} %all-gather.11.cloned.1.call-done, bf16[256,2048]{1,0:T(8,128)(2,1)S(1)} %multiply_convert_fusion, bf16[2048,1024]{1,0:T(8,128)(2,1)} %all-gather.9.cloned.1.call-done), kind=kOutput, calls=%fused_computation.37 | convolution fusion | flops 2148794368 | bytes 10485760 | tf_op jit(solution)/shard_map/dot_general | solution.py:122
  322.3 23.5 %reduce-scatter.2.cloned.1.call-done = bf16[64,2048]{1,0:T(8,128)(2,1)} async-done(((bf16[256,2048]{1,0:T(8,128)(2,1)}), bf16[64,2048]{1,0:T(8,128)(2,1)}) %reduce-scatter.2.cloned.1.call-update) | async-done | bytes 262160 | tf_op jit(solution)/shard_map/reduce_scatter | solution.py:121
  345.8 1.7 add_convert_fusion
  (58 shorter events, 0.7 us)
Async XLA Ops:
  6.5 120.7 %copy-start = (bf16[256,2048]{1,0:T(8,128)(2,1)S(1)}, bf16[256,2048]{1,0:T(8,128)(2,1)}, u32[]{:S(2)}) copy-start(bf16[256,2048]{1,0:T(8,128)(2,1)} %param.22) | copy-start | bytes 3145732
  6.5 74.1 %all-gather.7.cloned.1.call-start = ((), (), s32[]{:S(2)}) async-start(), calls=%async_computation.2 | async-start | bytes 1179648 | tf_op jit(solution)/shard_map/all_gather | solution.py:76
  7.3 122.7 %all-gather.5.cloned.1.call-start = ((), (), s32[]{:S(2)}) async-start(), calls=%async_computation.1 | async-start | bytes 1310720 | tf_op jit(solution)/shard_map/all_gather | solution.py:109
  8.0 157.4 %all-reduce.2.cloned.1.call-start = ((), (), s32[]{:S(2)}) async-start(), calls=%async_computation.3 | async-start | bytes 2097152 | tf_op jit(solution)/shard_map/psum | solution.py:106
  86.3 4.7 %copy-start.3 = (f32[256,2]{0,1:T(2,128)S(1)}, f32[256,2]{0,1:T(2,128)}, u32[]{:S(2)}) copy-start(f32[256,2]{0,1:T(2,128)} %get-tuple-element.265) | copy-start | bytes 6148 | tf_op jit(solution)/shard_map/while
  96.2 4.9 %copy-start.3 = (f32[256,2]{0,1:T(2,128)S(1)}, f32[256,2]{0,1:T(2,128)}, u32[]{:S(2)}) copy-start(f32[256,2]{0,1:T(2,128)} %get-tuple-element.265) | copy-start | bytes 6148 | tf_op jit(solution)/shard_map/while
  107.3 4.9 %copy-start.3 = (f32[256,2]{0,1:T(2,128)S(1)}, f32[256,2]{0,1:T(2,128)}, u32[]{:S(2)}) copy-start(f32[256,2]{0,1:T(2,128)} %get-tuple-element.265) | copy-start | bytes 6148 | tf_op jit(solution)/shard_map/while
  118.4 4.9 %copy-start.3 = (f32[256,2]{0,1:T(2,128)S(1)}, f32[256,2]{0,1:T(2,128)}, u32[]{:S(2)}) copy-start(f32[256,2]{0,1:T(2,128)} %get-tuple-element.265) | copy-start | bytes 6148 | tf_op jit(solution)/shard_map/while
  128.7 113.7 %all-gather.11.cloned.1.call-start = ((), (), s32[]{:S(2)}) async-start(), calls=%async_computation.5 | async-start | bytes 4718592 | tf_op jit(solution)/shard_map/all_gather | solution.py:119
  129.3 186.1 %all-gather.9.cloned.1.call-start = ((), (), s32[]{:S(2)}) async-start(), calls=%async_computation.4 | async-start | bytes 4718592 | tf_op jit(solution)/shard_map/all_gather | solution.py:116
  129.4 38.6 %copy-start.4 = (f32[2048]{0:T(1024)S(1)}, f32[2048]{0:T(1024)}, u32[]{:S(2)}) copy-start(f32[2048]{0:T(1024)} %param.23) | copy-start | bytes 24580
  129.9 215.9 %reduce-scatter.2.cloned.1.call-start = ((), (), s32[]{:S(2)}) async-start(), calls=%async_computation.6 | async-start | bytes 1310720 | tf_op jit(solution)/shard_map/reduce_scatter | solution.py:121
  130.0 37.5 %copy-start.1 = (bf16[256,2048]{1,0:T(8,128)(2,1)S(1)}, bf16[256,2048]{1,0:T(8,128)(2,1)}, u32[]{:S(2)}) copy-start(bf16[256,2048]{1,0:T(8,128)(2,1)} %all-gather.5.cloned.1.call-done) | copy-start | bytes 3145732
  165.4 2.0 copy-start.2
Sparse Core Ops, SparseCore 0:
  9.5 45.4 all-gather.6
  56.5 15.4 all-gather.4
  128.9 36.5 all-reduce.1
  167.3 75.0 all-gather.10
  244.4 70.9 all-gather.8
  322.4 23.2 reduce-scatter.1
where the time goes:
time: 355 us; the launch traced here: 354 us
  waiting for transfers between devices  208 us (59%)
  blocking collectives  65.8 us (19%)
  matrix products  33 us (9%)
  local copies, waits for them, and re-layouts  20.2 us (6%)
  between operations  13.7 us (4%)
  other arithmetic  12.9 us (4%)
    all_gather x1, waiting for transfers between devices, local(): down_full = lax.all_gather(down_weight, 'sp', axis=1, tiled=True)  74 us
    all_gather x1, waiting for transfers between devices, local(): lax.all_gather(up_weight, 'sp', axis=0, tiled=True)  73 us
    psum x1, waiting for transfers between devices, local(): lax.psum(jnp.dot(flat, out_weight, preferred_element_type=jnp.float32).as...  35.5 us
    all_gather x1, blocking collectives, local(): piece_b = lax.all_gather(key_b, 'sp', axis=0, tiled=True)  34.2 us
    all_gather x1, blocking collectives, local(): piece_a = lax.all_gather(key_a, 'sp', axis=0, tiled=True)  31.6 us
    reduce_scatter x1, waiting for transfers between devices, local(): lax.psum_scatter(jnp.dot(hidden, down_full, preferred_element_type=jnp.fl...  23.5 us
    dot_general x8, matrix products, absorb(): jnp.einsum('qhk,khe->qhe', weights.astype(jnp.bfloat16), vals, preferred_...  14.6 us
    dynamic_slice x8, local copies, waits for them, and re-layouts, local(): state_a, state_b = lax.scan(advance, (start_state, start_state), items)[0]  11.8 us
  transfers between devices with their start and end apart: 6, of which 4 were waited for; matrix products, arithmetic and copies ran while one was open for 16% of the time, Pallas kernels for 0%

commit v1 on v0

--- a/solution.py
+++ b/solution.py
@@ -116,7 +116,10 @@
         lax.all_gather(up_weight, "sp", axis=0, tiled=True),
         preferred_element_type=jnp.float32,
     )
-    down_full = lax.all_gather(down_weight, "sp", axis=1, tiled=True)
+    size = lax.axis_size("sp")
+    parts = jnp.stack([down_weight for _ in range(size)])
+    parts = lax.all_to_all(parts, "sp", split_axis=0, concat_axis=0)
+    down_full = jnp.concatenate(parts, axis=1)
     hidden = jnp.square(jax.nn.relu(lifted)).astype(jnp.bfloat16)
     lowered = lax.psum_scatter(
         jnp.dot(hidden, down_full, preferred_element_type=jnp.float32).astype(jnp.bfloat16),

time: 355 us -> 309 us (0.87)
  waiting for transfers between devices: 208 us -> 155 us
  starting transfers between devices: 0.2 us -> 5.04 us
    all_to_all x0 -> x1, waiting for transfers between devices: none -> 97.4 us  [local(): parts = lax.all_to_all(parts, 'sp', split_axis=0, concat_axis=0)]
    all_gather x1 -> x0, waiting for transfers between devices: 74 us -> none  [local(): down_full = lax.all_gather(down_weight, 'sp', axis=1, tiled=True)]
    all_gather x1, waiting for transfers between devices: 73 us -> 3.25 us  [local(): lax.all_gather(up_weight, 'sp', axis=0, tiled=True)]
    psum x1, waiting for transfers between devices: 35.5 us -> 28.8 us  [local(): lax.psum(jnp.dot(flat, out_weight, preferred_element_type=jnp.float32).as...]
    all_to_all x0 -> x1, starting transfers between devices: none -> 4.89 us  [local(): parts = lax.all_to_all(parts, 'sp', split_axis=0, concat_axis=0)]
  transfers between devices with their start and end apart: 6 -> 6, of which waited for: 4 -> 4; matrix products, arithmetic and copies ran while one was open for 16% -> 20% of each run, Pallas kernels for 0% -> 0%
where the time goes in v1:
time: 309 us; the launch traced here: 308 us
  waiting for transfers between devices  155 us (50%)
  blocking collectives  65.8 us (21%)
  matrix products  33 us (11%)
  local copies, waits for them, and re-layouts  22.9 us (7%)
  between operations  13.4 us (4%)
  other arithmetic  12.9 us (4%)
  starting transfers between devices  5.04 us (2%)
    all_to_all x1, waiting for transfers between devices, local(): parts = lax.all_to_all(parts, 'sp', split_axis=0, concat_axis=0)  97.4 us
    all_gather x1, blocking collectives, local(): piece_a = lax.all_gather(key_a, 'sp', axis=0, tiled=True)  34.2 us
    all_gather x1, blocking collectives, local(): piece_b = lax.all_gather(key_b, 'sp', axis=0, tiled=True)  31.6 us
    psum x1, waiting for transfers between devices, local(): lax.psum(jnp.dot(flat, out_weight, preferred_element_type=jnp.float32).as...  28.8 us
    reduce_scatter x1, waiting for transfers between devices, local(): lax.psum_scatter(jnp.dot(hidden, down_full, preferred_element_type=jnp.fl...  23.7 us
    dot_general x8, matrix products, absorb(): jnp.einsum('qhk,khe->qhe', weights.astype(jnp.bfloat16), vals, preferred_...  14.6 us
    dynamic_slice x8, local copies, waits for them, and re-layouts, local(): state_a, state_b = lax.scan(advance, (start_state, start_state), items)[0]  11.8 us
    dot_general x8, matrix products, absorb(): jnp.einsum('qhe,khe->qhk', queries, keys, preferred_element_type=jnp.floa...  10.1 us
  transfers between devices with their start and end apart: 6, of which 4 were waited for; matrix products, arithmetic and copies ran while one was open for 20% of the time, Pallas kernels for 0%

profile of v1, /device:TPU:0, one launch (start us, length us, event | category | flops | bytes accessed | tf_op | source)
XLA Modules:
  0.0 308.4 jit_solution(15751025213946851446)
XLA Ops:
  6.5 0.7 all-gather.6.cloned.1.call-update
  7.3 0.7 all-gather.4.cloned.1.call-update
  8.1 0.9 copy.21
  9.1 0.9 copy.22
  10.0 0.9 copy.23
  11.0 0.9 copy.24
  11.9 0.2 multiply_cosine_fusion
  12.2 34.2 %all_gather.16 = bf16[2048,128]{0,1:T(8,128)(2,1)S(1)} all-gather(bf16[256,128]{0,1:T(8,128)(2,1)S(1)} %bitcast.69), channel_id=1, replica_groups=mesh['sp'=8,'tp'=4] {'sp'}, dimensions={0}, use_global_device_ids=true | all-gather | bytes 589824 | tf_op jit(solution)/shard_map/all_gather | solution.py:74
  46.4 0.4 reshape.139
  46.8 0.9 copy.25
  47.7 31.6 %all_gather.18 = bf16[2048,128]{0,1:T(8,128)(2,1)S(1)} all-gather(bf16[256,128]{0,1:T(8,128)(2,1)S(1)} %bitcast.70), channel_id=1, replica_groups=mesh['sp'=8,'tp'=4] {'sp'}, dimensions={0}, use_global_device_ids=true | all-gather | bytes 589824 | tf_op jit(solution)/shard_map/all_gather | solution.py:75
  79.3 0.4 reshape.145
  79.7 0.9 copy.27
  80.6 2.1 reshape.142
  82.7 42.6 %while.21 = (s32[]{:T(128)}, f32[256,2]{0,1:T(2,128)S(1)}, f32[256,2]{0,1:T(2,128)}, f32[256,2,128]{0,2,1:T(8,128)}, f32[256,2]{0,1:T(2,128)S(1)}, /*index=5*/f3...) while((s32[]{:T(128)}, f32[256,2]{0,1:T(2,128)S(1)}, ...), condition=%wide.region_5.6_spmd.clone, body=%wide.region_0.5_spmd.clone.sunk | while | flops 204870656 | bytes 9381043 | solution.py:96
  82.7 1.3 fusion.60
  84.0 0.2 fusion.65
  84.2 1.3 fusion.62
  85.5 0.2 fusion.64
  85.6 0.6 fusion.66
  86.3 1.8 constant_dynamic-slice_fusion.2
  88.1 1.1 copy.33
  89.2 1.7 fusion.68
  90.9 1.0 fusion.67
  92.0 1.3 fusion.60
  93.4 1.3 fusion.62
  94.7 0.2 fusion.64
  94.8 1.3 fusion.66
  96.2 1.8 constant_dynamic-slice_fusion.2
  98.0 1.1 copy.33
  99.1 2.0 fusion.68
  101.1 2.0 fusion.67
  103.1 1.3 fusion.60
  104.5 1.3 fusion.62
  105.8 0.2 fusion.64
  106.0 1.3 fusion.66
  107.3 1.8 constant_dynamic-slice_fusion.2
  109.1 1.1 copy.33
  110.2 2.0 fusion.68
  112.2 2.0 fusion.67
  114.2 1.3 fusion.60
  115.6 1.3 fusion.62
  116.9 0.2 fusion.64
  117.1 1.3 fusion.66
  118.4 1.8 constant_dynamic-slice_fusion.2
  120.2 1.1 copy.33
  121.4 2.0 fusion.68
  123.4 2.0 fusion.67
  125.3 1.2 multiply_reduce_fusion.1
  126.6 0.7 multiply_convert_fusion.1
  127.3 1.5 convolution_convert_fusion.1
  128.8 0.2 copy.28
  129.0 2.5 stack.2
  131.5 4.9 %all-to-all-start = ((bf16[8,1024,256]{1,2,0:T(8,128)(2,1)}), bf16[8,1024,256]{1,2,0:T(8,128)(2,1)}, u32[]{:S(2)}, u32[]{:S(2)}) async-start(bf16[8,1024,256]{1,2,0:T(8,128)(2,1)} %stack.2), calls=%async_computation | async-start | bytes 8388608 | tf_op jit(solution)/shard_map/all_to_all | solution.py:121
  136.5 0.5 all-gather.8.cloned.1.call-update
  137.1 28.8 %all-reduce.2.cloned.1.call-done = bf16[256,2048]{1,0:T(8,128)(2,1)} async-done(((bf16[256,2048]{1,0:T(8,128)(2,1)}), bf16[256,2048]{1,0:T(8,128)(2,1)}) %all-reduce.2.cloned.1.call-update) | async-done | bytes 1048592 | tf_op jit(solution)/shard_map/psum | solution.py:106
  165.9 2.0 fusion.25
  167.9 0.5 multiply_reduce_fusion
  168.4 0.5 multiply_convert_fusion
  168.9 97.4 %all-to-all-done = bf16[8,1024,256]{1,2,0:T(8,128)(2,1)} async-done(((bf16[8,1024,256]{1,2,0:T(8,128)(2,1)}), bf16[8,1024,256]{1,2,0:T(8,128)(2,1)}, u32[]{:S(2)}, u32[]{:S(2)}) %all-to-all-start) | async-done | bytes 4194336 | tf_op jit(solution)/shard_map/all_to_all | solution.py:121
  266.3 3.2 %all-gather.8.cloned.1.call-done = bf16[2048,1024]{1,0:T(8,128)(2,1)} async-done(((bf16[256,1024]{1,0:T(8,128)(2,1)}), bf16[2048,1024]{1,0:T(8,128)(2,1)}) %all-gather.8.cloned.1.call-update) | async-done | bytes 4194320 | tf_op jit(solution)/shard_map/all_gather | solution.py:116
  269.6 6.9 %convolution_convert_fusion = bf16[256,2048]{1,0:T(8,128)(2,1)} fusion(bf16[1024,2048]{0,1:T(8,128)(2,1)} %bitcast.8, bf16[256,2048]{1,0:T(8,128)(2,1)S(1)} %multiply_convert_fusion, bf16[2048,1024]{1,0:T(8,128)(2,1)} %all-gather.8.cloned.1.call-done), kind=kOutput, calls=%fused_computation.37 | convolution fusion | flops 2148794368 | bytes 10485760 | tf_op jit(solution)/shard_map/dot_general | solution.py:125
  276.5 23.7 %reduce-scatter.2.cloned.1.call-done = bf16[64,2048]{1,0:T(8,128)(2,1)} async-done(((bf16[256,2048]{1,0:T(8,128)(2,1)}), bf16[64,2048]{1,0:T(8,128)(2,1)}) %reduce-scatter.2.cloned.1.call-update) | async-done | bytes 262160 | tf_op jit(solution)/shard_map/reduce_scatter | solution.py:124
  300.2 1.7 add_convert_fusion
  (61 shorter events, 1.0 us)
Async XLA Ops:
  6.5 120.8 %copy-start = (bf16[256,2048]{1,0:T(8,128)(2,1)S(1)}, bf16[256,2048]{1,0:T(8,128)(2,1)}, u32[]{:S(2)}) copy-start(bf16[256,2048]{1,0:T(8,128)(2,1)} %param.22) | copy-start | bytes 3145732
  6.5 74.1 %all-gather.6.cloned.1.call-start = ((), (), s32[]{:S(2)}) async-start(), calls=%async_computation.3 | async-start | bytes 1179648 | tf_op jit(solution)/shard_map/all_gather | solution.py:76
  7.3 129.8 %all-gather.4.cloned.1.call-start = ((), (), s32[]{:S(2)}) async-start(), calls=%async_computation.2 | async-start | bytes 1310720 | tf_op jit(solution)/shard_map/all_gather | solution.py:109
  8.0 157.9 %all-reduce.2.cloned.1.call-start = ((), (), s32[]{:S(2)}) async-start(), calls=%async_computation.4 | async-start | bytes 2097152 | tf_op jit(solution)/shard_map/psum | solution.py:106
  86.3 4.7 %copy-start.4 = (f32[256,2]{0,1:T(2,128)S(1)}, f32[256,2]{0,1:T(2,128)}, u32[]{:S(2)}) copy-start(f32[256,2]{0,1:T(2,128)} %get-tuple-element.265) | copy-start | bytes 6148 | tf_op jit(solution)/shard_map/while
  96.2 4.9 %copy-start.4 = (f32[256,2]{0,1:T(2,128)S(1)}, f32[256,2]{0,1:T(2,128)}, u32[]{:S(2)}) copy-start(f32[256,2]{0,1:T(2,128)} %get-tuple-element.265) | copy-start | bytes 6148 | tf_op jit(solution)/shard_map/while
  107.3 4.9 %copy-start.4 = (f32[256,2]{0,1:T(2,128)S(1)}, f32[256,2]{0,1:T(2,128)}, u32[]{:S(2)}) copy-start(f32[256,2]{0,1:T(2,128)} %get-tuple-element.265) | copy-start | bytes 6148 | tf_op jit(solution)/shard_map/while
  118.4 4.9 %copy-start.4 = (f32[256,2]{0,1:T(2,128)S(1)}, f32[256,2]{0,1:T(2,128)}, u32[]{:S(2)}) copy-start(f32[256,2]{0,1:T(2,128)} %get-tuple-element.265) | copy-start | bytes 6148 | tf_op jit(solution)/shard_map/while
  125.3 3.5 %copy-start.3 = (bf16[1024,256]{1,0:T(8,128)(2,1)S(1)}, bf16[1024,256]{1,0:T(8,128)(2,1)}, u32[]{:S(2)}) copy-start(bf16[1024,256]{1,0:T(8,128)(2,1)} %param.25) | copy-start | bytes 1572868
  131.5 134.8 %all-to-all-start = ((bf16[8,1024,256]{1,2,0:T(8,128)(2,1)}), bf16[8,1024,256]{1,2,0:T(8,128)(2,1)}, u32[]{:S(2)}, u32[]{:S(2)}) async-start(bf16[8,1024,256]{1,2,0:T(8,128)(2,1)} %stack.2), calls=%async_computation | async-start | bytes 8388608 | tf_op jit(solution)/shard_map/all_to_all | solution.py:121
  136.4 133.2 %all-gather.8.cloned.1.call-start = ((), (), s32[]{:S(2)}) async-start(), calls=%async_computation.5 | async-start | bytes 4718592 | tf_op jit(solution)/shard_map/all_gather | solution.py:116
  136.4 32.0 %copy-start.5 = (f32[2048]{0:T(1024)S(1)}, f32[2048]{0:T(1024)}, u32[]{:S(2)}) copy-start(f32[2048]{0:T(1024)} %param.23) | copy-start | bytes 24580
  137.0 163.2 %reduce-scatter.2.cloned.1.call-start = ((), (), s32[]{:S(2)}) async-start(), calls=%async_computation.6 | async-start | bytes 1310720 | tf_op jit(solution)/shard_map/reduce_scatter | solution.py:124
  137.0 30.8 %copy-start.1 = (bf16[256,2048]{1,0:T(8,128)(2,1)S(1)}, bf16[256,2048]{1,0:T(8,128)(2,1)}, u32[]{:S(2)}) copy-start(bf16[256,2048]{1,0:T(8,128)(2,1)} %all-gather.4.cloned.1.call-done) | copy-start | bytes 3145732
  165.9 2.0 copy-start.2
Sparse Core Ops, SparseCore 0:
  9.5 45.4 all-gather.5
  56.5 15.4 all-gather.3
  128.9 36.9 all-reduce.1
  167.9 101.6 all-gather.7
  276.6 23.5 reduce-scatter.1
